TPU v7x, 32 devices: a whole 2x2x4 slice. The times are simulated.
32 devices in a mesh: grp: 2 (over y), kv: 4 (over z), tp: 4 (over x, core).
Axes of the slice: x: 2, y: 2, z: 4, core: 2. Of those that a mesh axis runs over, the one named last changes fastest.
Arguments:
- tokens: bfloat16 [48, 4096], P('grp', ('kv', 'tp')), parts along dimension 0, may hold values from -30 to 30
- norm_gain: bfloat16 [4096], P(('kv', 'tp')), may hold values from 0.099609375 to 1.8984375
- query_weight: bfloat16 [4096, 4096], P('kv', 'tp'), may hold values from -0.09375 to 0.09375
- key_weight: bfloat16 [4096, 4096], P('kv', 'tp'), may hold values from -0.5 to 0.5
- value_weight: bfloat16 [4096, 4096], P('kv', 'tp'), may hold values from -0.09375 to 0.09375
- lambda_head: float32 [16], P('tp'), may hold values from 0.3 to 0.8
- head_gain: float32 [256], replicated, may hold values from 0.1 to 1.9
- out_weight: bfloat16 [4096, 4096], P('tp', 'kv'), may hold values from -0.09375 to 0.09375
- cache_keys: bfloat16 [48, 256, 4096], P('grp', 'kv', 'tp'), parts along dimension 0, may hold values from -300 to 300
- cache_values: bfloat16 [48, 256, 4096], P('grp', 'kv', 'tp'), parts along dimension 0, may hold values from -6 to 6
- lengths: int32 [48], P('grp'), parts along dimension 0, may hold values from 64 to 255, as said below
Outputs:
- layer_out: bfloat16 [48, 4096], P('grp', ('kv', 'tp')), parts along dimension 0
- log_sums: float32 [48, 16, 2], P('grp', 'tp'), parts along dimension 0
There are 2 independent parts, one for each index of `grp`. A program takes and returns all parts, laid end to end along the dimension named above; an argument that names none is the same for every part. Nothing has to cross between parts.
Inputs may be any that keep to these rules, and one draw needn't show every extreme that they name: The new token of sequence b goes to cache position lengths[b]; in every draw some sequence has the largest length allowed.
All inputs are finite; a program needn't handle non-finite values.
Results may differ from a plain program's by a relative error of at most 0.017.
The roundings to bfloat16 on the way count: a program that leaves them out, or rounds other values in their place, can miss the bound.
Values may be sent and summed in bfloat16 or wider, within the bound.
A program may use at most 64 MiB of HBM per device.

v0:
```python
import functools
import math

import jax
import jax.numpy as jnp
from jax import lax
from jax.experimental import pallas as pl
from jax.experimental.pallas import tpu as pltpu
from jax.sharding import PartitionSpec as P

D = 4096
HEAD_DIM = 128
VALUE_DIM = 256


def merged(part, axis, combine):
    gathered = jax.tree.map(lambda a: lax.all_gather(a, axis), part)

    def take(source):
        return jax.tree.map(lambda a: lax.dynamic_index_in_dim(a, source, 0, False), gathered)

    return lax.fori_loop(
        1, lax.axis_size(axis), lambda source, state: combine(state, take(source)), take(0)
    )


def rotate(vectors, lengths):
    half_dim = vectors.shape[-1] // 2
    freqs = jnp.power(
        jnp.float32(500000.0), -(jnp.arange(half_dim, dtype=jnp.float32) * 2.0 / vectors.shape[-1])
    )
    angles = lengths.astype(jnp.float32)[:, None] * freqs[None, :]
    cosine = jnp.cos(angles)[:, None, None, :]
    sine = jnp.sin(angles)[:, None, None, :]
    lower = vectors[..., :half_dim]
    upper = vectors[..., half_dim:]
    return jnp.concatenate([lower * cosine - upper * sine, upper * cosine + lower * sine], axis=-1)


def fold_maps(left_part, right_part):
    left_max, left_sum, left_out = left_part
    right_max, right_sum, right_out = right_part
    joint = jnp.maximum(left_max, right_max)
    left_scale = jnp.exp(left_max - joint)
    right_scale = jnp.exp(right_max - joint)
    return (
        joint,
        left_sum * left_scale + right_sum * right_scale,
        left_out * left_scale[..., None] + right_out * right_scale[..., None],
    )


def on_device(
    tokens,
    norm_gain,
    query_weight,
    key_weight,
    value_weight,
    lambda_head,
    head_gain,
    out_weight,
    cache_keys,
    cache_values,
    lengths,
):
    seq_count = tokens.shape[0]
    heads_loc = lambda_head.shape[0]
    token_block, gain_block = (
        lax.all_gather(tokens, "tp", axis=1, tiled=True),
        lax.all_gather(norm_gain, "tp", axis=0, tiled=True),
    )
    tok_float = token_block.astype(jnp.float32)
    scaled = (tok_float * gain_block.astype(jnp.float32)).astype(jnp.bfloat16)
    query_part = jnp.dot(scaled, query_weight, preferred_element_type=jnp.float32)
    key_part = jnp.dot(scaled, key_weight, preferred_element_type=jnp.float32)
    value_part = jnp.dot(scaled, value_weight, preferred_element_type=jnp.float32)
    local_squares = jnp.sum(tok_float * tok_float, axis=1)
    query_sum, key_sum, value_sum, row_squares = lax.psum(
        (query_part, key_part, value_part, local_squares), "kv"
    )
    inv_rms = lax.rsqrt(row_squares / D + 1e-06)[:, None]
    queries = rotate(
        (query_sum * inv_rms).reshape(seq_count, heads_loc, 2, HEAD_DIM), lengths
    ).astype(jnp.bfloat16)
    key_new = rotate(
        (key_sum * inv_rms).reshape(seq_count, heads_loc, 2, HEAD_DIM), lengths
    ).astype(jnp.bfloat16)
    value_new = (value_sum * inv_rms).astype(jnp.bfloat16).reshape(seq_count, heads_loc, VALUE_DIM)
    span_len = cache_keys.shape[1]
    positions = lax.axis_index("kv") * span_len + jnp.arange(span_len, dtype=jnp.int32)
    new_slot = positions[None, :] == lengths[:, None]
    before = positions[None, :] < lengths[:, None]
    visible = positions[None, :] <= lengths[:, None]
    score_scale = HEAD_DIM ** (-0.5)
    keys_four = cache_keys.reshape(seq_count, span_len, heads_loc, 2, HEAD_DIM)
    scores = (
        jnp.einsum("bhcd,bphcd->bhcp", queries, keys_four, preferred_element_type=jnp.float32)
        * score_scale
    )
    new_score = (
        jnp.einsum("bhcd,bhcd->bhc", queries, key_new, preferred_element_type=jnp.float32)
        * score_scale
    )
    scores = jnp.where(new_slot[:, None, None, :], new_score[..., None], scores)
    visible_four = visible[:, None, None, :]
    block_max = jnp.max(jnp.where(visible_four, scores, -1e30), axis=-1)
    weights = jnp.where(visible_four, jnp.exp(scores - block_max[..., None]), 0.0)
    block_sum = jnp.sum(weights, axis=-1)
    weights_low = weights.astype(jnp.bfloat16)
    cache_weights = jnp.where(before[:, None, None, :], weights_low, jnp.zeros((), jnp.bfloat16))
    values_four = cache_values.reshape(seq_count, span_len, heads_loc, VALUE_DIM)
    block_out = jnp.einsum(
        "bhcp,bphe->bhce", cache_weights, values_four, preferred_element_type=jnp.float32
    )
    weight_new = jnp.sum(
        jnp.where(new_slot[:, None, None, :], weights_low.astype(jnp.float32), 0.0), axis=-1
    )
    block_out = block_out + weight_new[..., None] * value_new.astype(jnp.float32)[:, :, None, :]
    row_max, weight_total, combined = merged((block_max, block_sum, block_out), "kv", fold_maps)
    map_out = combined / weight_total[..., None]
    difference = map_out[:, :, 0] - lambda_head[None, :, None] * map_out[:, :, 1]
    inv_head = lax.rsqrt(jnp.mean(difference * difference, axis=-1, keepdims=True) + 1e-05)
    attended = (
        (difference * inv_head * head_gain)
        .astype(jnp.bfloat16)
        .reshape(seq_count, heads_loc * VALUE_DIM)
    )
    log_sums = row_max + jnp.log(weight_total)
    partial_value = jnp.dot(attended, out_weight, preferred_element_type=jnp.float32)
    layer_out = lax.psum_scatter(
        partial_value.astype(jnp.bfloat16), "tp", scatter_dimension=1, tiled=True
    )
    return (layer_out, log_sums)


MESH = pl.DeviceIdType.MESH
LANES = 128
ROWS = 8


def fused_kernel(
    n_kv,
    n_tp,
    tok_hbm,
    gain_hbm,
    wq_hbm,
    wk_hbm,
    wv_hbm,
    lam_ref,
    hgain_ref,
    wo_hbm,
    ck_hbm,
    cv_hbm,
    len_ref,
    out_ref,
    log_ref,
    tok_buf,
    gain_buf,
    scaled_buf,
    w_buf,
    k_buf,
    v_buf,
    wo_buf,
    part_send,
    part_recv,
    q_send,
    q_recv,
    att_send,
    att_recv,
    head_buf,
    log_send,
    log_recv,
    o_send,
    o_recv,
    own_sem,
    w_sem,
    kv_sem,
    wo_sem,
    tok_ss,
    tok_rs,
    part_ss,
    part_rs,
    q_ss,
    q_rs,
    att_ss,
    att_rs,
    head_ss,
    head_rs,
    o_ss,
    o_rs,
):
    f32, bf16 = jnp.float32, jnp.bfloat16
    my_kv, my_tp = lax.axis_index("kv"), lax.axis_index("tp")
    seqs, tok_w = tok_hbm.shape
    span = ck_hbm.shape[1]
    vdim = VALUE_DIM
    out_w = out_ref.shape[1]

    def kv_at(offset):
        return lax.rem(my_kv + offset, n_kv)

    def tp_at(offset):
        return lax.rem(my_tp + offset, n_tp)

    def send(src, dst, ss, rs, axis, peer):
        copy = pltpu.make_async_remote_copy(
            src_ref=src, dst_ref=dst, send_sem=ss, recv_sem=rs, device_id={axis: peer}, device_id_type=MESH
        )
        copy.start()
        return copy

    barrier = pltpu.get_barrier_semaphore()
    for offset in range(1, n_tp):
        pl.semaphore_signal(barrier, inc=1, device_id={"tp": tp_at(offset)}, device_id_type=MESH)
    for offset in range(1, n_kv):
        pl.semaphore_signal(barrier, inc=1, device_id={"kv": kv_at(offset)}, device_id_type=MESH)

    def load(src, dst, sem):
        copy = pltpu.make_async_copy(src, dst, sem)
        copy.start()
        return copy

    own_loads = [
        load(tok_hbm, tok_buf.at[my_tp], own_sem.at[0]),
        load(gain_hbm, gain_buf.at[my_tp], own_sem.at[1]),
    ]
    w_loads = []
    for i in range(n_kv):
        cols = pl.ds(pl.multiple_of(kv_at(i + 1) * vdim, vdim), vdim)
        w_loads.append(
            [
                load(w.at[:, cols], w_buf.at[i, :, pl.ds(m * vdim, vdim)], w_sem.at[i * 3 + m])
                for m, w in enumerate((wq_hbm, wk_hbm, wv_hbm))
            ]
        )
    order = [n_kv - 1] + list(range(n_kv - 1))
    kv_loads = {}
    for i in order:
        cols = pl.ds(pl.multiple_of(kv_at(i + 1) * vdim, vdim), vdim)
        kv_loads[i] = (
            load(ck_hbm.at[:, :, cols], k_buf.at[i], kv_sem.at[2 * i]),
            load(cv_hbm.at[:, :, cols], v_buf.at[i], kv_sem.at[2 * i + 1]),
        )
    wo_loads = []
    for i in range(n_tp):
        cols = pl.ds(pl.multiple_of(tp_at(i + 1) * out_w, out_w), out_w)
        wo_loads.append(load(wo_hbm.at[:, cols], wo_buf.at[i], wo_sem.at[i]))

    pl.semaphore_wait(barrier, n_tp + n_kv - 2)

    tok_copies = []
    for o in range(1, n_tp):
        peer = tp_at(o)
        tok_copies.append(
            send(tok_hbm, tok_buf.at[my_tp], tok_ss.at[2 * o - 2], tok_rs.at[2 * o - 2], "tp", peer)
        )
        tok_copies.append(
            send(gain_hbm, gain_buf.at[my_tp], tok_ss.at[2 * o - 1], tok_rs.at[2 * o - 1], "tp", peer)
        )

    row_id = lax.broadcasted_iota(jnp.int32, (seqs, LANES), 0)
    lens = jnp.zeros((seqs, LANES), jnp.int32)
    for b in range(seqs):
        lens = jnp.where(row_id == b, len_ref[b], lens)
    lane_id = lax.broadcasted_iota(jnp.int32, (seqs, LANES), 1)
    half = HEAD_DIM // 2
    upper = lane_id >= half
    freq_id = jnp.where(upper, lane_id - half, lane_id).astype(f32)
    angles = lens.astype(f32) * jnp.exp(freq_id * (-2.0 * math.log(500000.0) / HEAD_DIM))
    cosine = jnp.cos(angles)
    sine = jnp.sin(angles)
    sine = jnp.where(upper, sine, -sine)

    for copy in own_loads:
        copy.wait()
    for copy in tok_copies:
        copy.wait_recv()
    squares = jnp.zeros((seqs, 1), f32)
    for s in range(n_tp):
        tok = tok_buf[s].astype(f32)
        squares = squares + jnp.sum(tok * tok, axis=1, keepdims=True)
        scaled_buf[:, s * tok_w : (s + 1) * tok_w] = (tok * gain_buf[s].astype(f32)).astype(bf16)
    scaled = scaled_buf[...]

    part_copies = []
    for i in range(n_kv):
        for copy in w_loads[i]:
            copy.wait()
        part = jnp.dot(scaled, w_buf[i], preferred_element_type=f32)
        if i < n_kv - 1:
            part_send[i, :, : 3 * vdim] = part
            part_send[i, :, 3 * vdim :] = jnp.broadcast_to(squares, (seqs, LANES))
            part_copies.append(
                send(part_send.at[i], part_recv.at[i], part_ss.at[i], part_rs.at[i], "kv", kv_at(i + 1))
            )
    total, sq_total = part, squares
    for i, copy in enumerate(part_copies):
        copy.wait_recv()
        total = total + part_recv[i, :, : 3 * vdim]
        sq_total = sq_total + part_recv[i, :, 3 * vdim : 3 * vdim + 1]
    total = total * lax.rsqrt(sq_total / (tok_w * n_tp * n_kv) + 1e-06)

    def rotated(x):
        return (x * cosine + pltpu.roll(x, half, 1) * sine).astype(bf16)

    q_maps = [rotated(total[:, c * HEAD_DIM : (c + 1) * HEAD_DIM]) for c in range(2)]
    for c in range(2):
        q_send[:, c * HEAD_DIM : (c + 1) * HEAD_DIM] = q_maps[c]
    q_copies = [
        send(q_send, q_recv.at[o - 1], q_ss.at[o - 1], q_rs.at[o - 1], "kv", kv_at(o)) for o in range(1, n_kv)
    ]
    score_scale = HEAD_DIM ** (-0.5)
    new_scores = []
    for c in range(2):
        k_new = rotated(total[:, vdim + c * HEAD_DIM : vdim + (c + 1) * HEAD_DIM])
        new_scores.append(
            jnp.sum(q_maps[c].astype(f32) * k_new.astype(f32), axis=1, keepdims=True) * score_scale
        )
    new_score = jnp.concatenate(new_scores, axis=0)
    v_new = total[:, 2 * vdim :].astype(bf16).astype(f32)
    v_new = jnp.concatenate([v_new, v_new], axis=0)

    wide = ROWS * span
    col = lax.broadcasted_iota(jnp.int32, (2 * ROWS, wide), 1)
    row = lax.broadcasted_iota(jnp.int32, (2 * ROWS, wide), 0)
    start = (row % ROWS) * span
    masks = []
    for g in range(seqs // ROWS):
        len_g = lens[g * ROWS : (g + 1) * ROWS, 0:1]
        len_g = jnp.concatenate([len_g, len_g], axis=0)
        limit = jnp.minimum(len_g - my_kv * span, span)
        masks.append((col >= start) & (col - start < limit))
    lane_q = lax.broadcasted_iota(jnp.int32, (ROWS, vdim), 1)
    stat_lane = lax.broadcasted_iota(jnp.int32, (2 * ROWS, LANES), 1)
    contract_last = (((1,), (1,)), ((), ()))
    att_copies = []
    for i in order:
        kv_loads[i][0].wait()
        kv_loads[i][1].wait()
        if i == n_kv - 1:
            q_head = q_send[...]
        else:
            slot = n_kv - 2 - i
            q_copies[slot].wait_recv()
            q_head = q_recv[slot]
        q_float = q_head.astype(f32)
        for g in range(seqs // ROWS):
            rows = slice(g * ROWS, (g + 1) * ROWS)
            q_g = q_float[rows]
            lhs = jnp.concatenate(
                [jnp.where(lane_q < HEAD_DIM, q_g, 0.0), jnp.where(lane_q < HEAD_DIM, 0.0, q_g)], axis=0
            ).astype(bf16)
            keys = k_buf[i, rows].reshape(wide, vdim)
            scores = lax.dot_general(lhs, keys, contract_last, preferred_element_type=f32) * score_scale
            scores = jnp.where(masks[g], scores, -1e30)
            top = jnp.max(scores, axis=1, keepdims=True)
            weights = jnp.where(masks[g], jnp.exp(scores - top), 0.0)
            mass = jnp.sum(weights, axis=1, keepdims=True)
            values = v_buf[i, rows].reshape(wide, vdim)
            out = jnp.dot(weights.astype(bf16), values, preferred_element_type=f32)
            stats = jnp.where(stat_lane < LANES // 2, top, mass)
            for c in range(2):
                dst = slice(c * seqs + g * ROWS, c * seqs + (g + 1) * ROWS)
                att_send[i, dst, :vdim] = out[c * ROWS : (c + 1) * ROWS]
                att_send[i, dst, vdim:] = stats[c * ROWS : (c + 1) * ROWS]
        if i < n_kv - 1:
            att_copies.append(
                send(att_send.at[i], att_recv.at[i], att_ss.at[i], att_rs.at[i], "kv", kv_at(i + 1))
            )

    for copy in att_copies:
        copy.wait_recv()
    blocks = [att_send[n_kv - 1]] + [att_recv[i] for i in range(n_kv - 1)]
    mid = vdim + LANES // 2
    row_max = new_score
    for block in blocks:
        row_max = jnp.maximum(row_max, block[:, vdim : vdim + 1])
    new_weight = jnp.exp(new_score - row_max)
    weight_total = new_weight
    combined = new_weight * v_new
    for block in blocks:
        scale = jnp.exp(block[:, vdim : vdim + 1] - row_max)
        weight_total = weight_total + scale * block[:, mid : mid + 1]
        combined = combined + scale * block[:, :vdim]
    map_out = combined / weight_total
    difference = map_out[:seqs] - lam_ref[my_kv] * map_out[seqs:]
    inv_head = lax.rsqrt(jnp.mean(difference * difference, axis=1, keepdims=True) + 1e-05)
    head_buf[my_kv] = (difference * inv_head * hgain_ref[...]).astype(bf16)
    head_copies = [
        send(head_buf.at[my_kv], head_buf.at[my_kv], head_ss.at[o - 1], head_rs.at[o - 1], "kv", kv_at(o))
        for o in range(1, n_kv)
    ]
    logs = row_max + jnp.log(weight_total)
    own_logs = jnp.where(
        lane_id == 2 * my_kv, logs[:seqs], jnp.where(lane_id == 2 * my_kv + 1, logs[seqs:], 0.0)
    )
    log_send[...] = own_logs
    log_copies = [
        send(log_send, log_recv.at[o - 1], head_ss.at[n_kv - 2 + o], head_rs.at[n_kv - 2 + o], "kv", kv_at(o))
        for o in range(1, n_kv)
    ]

    for copy in wo_loads:
        copy.wait()
    for copy in head_copies:
        copy.wait_recv()
    attended = jnp.concatenate([head_buf[h] for h in range(n_kv)], axis=1)
    o_copies = []
    for i in range(n_tp):
        part = jnp.dot(attended, wo_buf[i], preferred_element_type=f32).astype(bf16)
        if i < n_tp - 1:
            o_send[i] = part
            o_copies.append(send(o_send.at[i], o_recv.at[i], o_ss.at[i], o_rs.at[i], "tp", tp_at(i + 1)))
    for i, copy in enumerate(log_copies):
        copy.wait_recv()
        own_logs = own_logs + log_recv[i]
    log_ref[...] = own_logs
    result = part.astype(f32)
    for i, copy in enumerate(o_copies):
        copy.wait_recv()
        result = result + o_recv[i].astype(f32)
    out_ref[...] = result.astype(bf16)
    for copy in tok_copies + part_copies + q_copies + att_copies + head_copies + log_copies + o_copies:
        copy.wait_send()


def fused(
    n_kv,
    n_tp,
    tokens,
    norm_gain,
    query_weight,
    key_weight,
    value_weight,
    lambda_head,
    head_gain,
    out_weight,
    cache_keys,
    cache_values,
    lengths,
):
    seqs, tok_w = tokens.shape
    span = cache_keys.shape[1]
    depth = query_weight.shape[0]
    heads = lambda_head.shape[0]
    out_w = out_weight.shape[1] // n_tp
    bf16, f32 = jnp.bfloat16, jnp.float32
    dma = pltpu.SemaphoreType.DMA
    anyspace = pl.BlockSpec(memory_space=pl.ANY)
    vmem = pl.BlockSpec(memory_space=pltpu.VMEM)
    smem = pl.BlockSpec(memory_space=pltpu.SMEM)
    k1, t1 = n_kv - 1, n_tp - 1
    layer, logs = pl.pallas_call(
        functools.partial(fused_kernel, n_kv, n_tp),
        out_shape=(
            jax.ShapeDtypeStruct((seqs, out_w), bf16),
            jax.ShapeDtypeStruct((seqs, LANES), f32),
        ),
        in_specs=[anyspace] * 5 + [smem, vmem] + [anyspace] * 3 + [smem],
        out_specs=(vmem, vmem),
        scratch_shapes=[
            pltpu.VMEM((n_tp, seqs, tok_w), bf16),
            pltpu.VMEM((n_tp, 1, tok_w), bf16),
            pltpu.VMEM((seqs, depth), bf16),
            pltpu.VMEM((n_kv, depth, 3 * VALUE_DIM), bf16),
            pltpu.VMEM((n_kv, seqs, span, VALUE_DIM), bf16),
            pltpu.VMEM((n_kv, seqs, span, VALUE_DIM), bf16),
            pltpu.VMEM((n_tp, out_weight.shape[0], out_w), bf16),
            pltpu.VMEM((k1, seqs, 3 * VALUE_DIM + LANES), f32),
            pltpu.VMEM((k1, seqs, 3 * VALUE_DIM + LANES), f32),
            pltpu.VMEM((seqs, VALUE_DIM), bf16),
            pltpu.VMEM((k1, seqs, VALUE_DIM), bf16),
            pltpu.VMEM((n_kv, 2 * seqs, VALUE_DIM + LANES), f32),
            pltpu.VMEM((k1, 2 * seqs, VALUE_DIM + LANES), f32),
            pltpu.VMEM((n_kv, seqs, VALUE_DIM), bf16),
            pltpu.VMEM((seqs, LANES), f32),
            pltpu.VMEM((k1, seqs, LANES), f32),
            pltpu.VMEM((t1, seqs, out_w), bf16),
            pltpu.VMEM((t1, seqs, out_w), bf16),
            dma((2,)),
            dma((3 * n_kv,)),
            dma((2 * n_kv,)),
            dma((n_tp,)),
            dma((2 * t1,)),
            dma((2 * t1,)),
            dma((k1,)),
            dma((k1,)),
            dma((k1,)),
            dma((k1,)),
            dma((k1,)),
            dma((k1,)),
            dma((2 * k1,)),
            dma((2 * k1,)),
            dma((t1,)),
            dma((t1,)),
        ],
        compiler_params=pltpu.CompilerParams(
            collective_id=0, has_side_effects=True, vmem_limit_bytes=60 * 1024 * 1024
        ),
        name="decode_step",
    )(
        tokens,
        norm_gain.reshape(1, tok_w),
        query_weight,
        key_weight,
        value_weight,
        lambda_head,
        head_gain.reshape(1, VALUE_DIM),
        out_weight,
        cache_keys,
        cache_values,
        lengths,
    )
    return layer, logs[:, : 2 * heads].reshape(seqs, heads, 2)


def fits_fused(n_kv, n_tp, tokens, lambda_head, out_weight, cache_keys):
    seqs, tok_w = tokens.shape
    heads = lambda_head.shape[0]
    resident = 2 * (4 * out_weight.size + 2 * cache_keys.size)
    return (
        heads == n_kv
        and n_kv > 1
        and n_tp > 1
        and seqs % ROWS == 0
        and tok_w % LANES == 0
        and (out_weight.shape[1] // n_tp) % LANES == 0
        and 2 * heads <= LANES
        and cache_keys.shape[1] % 16 == 0
        and resident <= 40 * 1024 * 1024
    )


def step(*args):
    n_kv, n_tp = lax.axis_size("kv"), lax.axis_size("tp")
    tokens, lambda_head, out_weight, cache_keys = args[0], args[5], args[7], args[8]
    if fits_fused(n_kv, n_tp, tokens, lambda_head, out_weight, cache_keys):
        return fused(n_kv, n_tp, *args)
    return on_device(*args)


def solution(mesh):
    in_specs = (
        P("grp", ("kv", "tp")),
        P(("kv", "tp")),
        P("kv", "tp"),
        P("kv", "tp"),
        P("kv", "tp"),
        P("tp"),
        P(),
        P("tp", "kv"),
        P("grp", "kv", "tp"),
        P("grp", "kv", "tp"),
        P("grp"),
    )
    out_specs = (P("grp", ("kv", "tp")), P("grp", "tp", None))
    return jax.shard_map(
        step, mesh=mesh, in_specs=in_specs, out_specs=out_specs, check_vma=False
    )
```

profile of v0, /device:TPU:0, one launch (start us, length us, event | category | flops | bytes accessed | tf_op | source)
XLA Modules:
  0.0 42.9 jit_solution(1194937400779228148)
XLA Ops:
  0.6 1.2 %reshape.13.gain_hbm = bf16[1,256]{1,0:T(2,128)(2,1)} reshape(bf16[256]{0:T(256)(128)(2,1)} %param.12) | data formatting | bytes 1024 | tf_op jit(solution)/shard_map/reshape | solution.py:503
  1.9 38.4 %decode_step.1 = (bf16[24,256]{1,0:T(8,128)(2,1)}, f32[24,128]{1,0:T(8,128)}) custom-call(bf16[24,256]{1,0:T(8,128)(2,1)} %tok_hbm.1, bf16[1,256]{1,0:T(2,128)(2,1)} %reshape.13.gain_hbm, bf16[1024,1024]{1,0:T(8,128)(2,1)} %wq_hbm.1, bf16[1024,1024]{1,0:T(8,128)(2,1)} %wk_hbm.1, bf16[1024,1024]{1,0:T(8,128)(2,1)} %wv_hbm.1, f32[4]{0:T(128)} %lam_ref.1, ...), custom_call_target="tpu_custom_call" | custom-call | tf_op jit(solution)/shard_map/decode_step/pallas_call | solution.py:453
  40.2 1.4 %copy.14 = f32[24,8]{0,1:T(8,128)} copy(f32[24,8]{1,0:T(8,128)} %bitcast.3) | data formatting | bytes 1536 | tf_op jit(solution)/shard_map/slice | solution.py:514
  41.6 1.3 %copy.16 = bf16[24,256]{1,0:T(8,128)(2,1)} copy(bf16[24,256]{1,0:T(8,128)(2,1)} %get-tuple-element.10) | data formatting | bytes 24576
where the time goes:
time: 43.2 us; the launch traced here: 42.9 us
  Pallas kernels  38.4 us (89%)
  local copies, waits for them, and re-layouts  3.89 us (9%)
  between operations  0.64 us (1%)
    pallas_call x1, Pallas kernels, fused(): pl.pallas_call(functools.partial(fused_kernel, n_kv, n_tp), out_shape=(ja...  38.4 us
    slice x1, local copies, waits for them, and re-layouts, fused(): return (layer, logs[:, :2 * heads].reshape(seqs, heads, 2))  1.37 us
    unnamed x1, local copies, waits for them, and re-layouts  1.31 us
    reshape x1, local copies, waits for them, and re-layouts, fused(): norm_gain.reshape(1, tok_w)  1.22 us

commit v1 on v0

v1 whole, which is shorter than its diff:
```python
import functools
import math

import jax
import jax.numpy as jnp
from jax import lax
from jax.experimental import pallas as pl
from jax.experimental.pallas import tpu as pltpu
from jax.sharding import PartitionSpec as P

D = 4096
HEAD_DIM = 128
VALUE_DIM = 256


def merged(part, axis, combine):
    gathered = jax.tree.map(lambda a: lax.all_gather(a, axis), part)

    def take(source):
        return jax.tree.map(lambda a: lax.dynamic_index_in_dim(a, source, 0, False), gathered)

    return lax.fori_loop(
        1, lax.axis_size(axis), lambda source, state: combine(state, take(source)), take(0)
    )


def rotate(vectors, lengths):
    half_dim = vectors.shape[-1] // 2
    freqs = jnp.power(
        jnp.float32(500000.0), -(jnp.arange(half_dim, dtype=jnp.float32) * 2.0 / vectors.shape[-1])
    )
    angles = lengths.astype(jnp.float32)[:, None] * freqs[None, :]
    cosine = jnp.cos(angles)[:, None, None, :]
    sine = jnp.sin(angles)[:, None, None, :]
    lower = vectors[..., :half_dim]
    upper = vectors[..., half_dim:]
    return jnp.concatenate([lower * cosine - upper * sine, upper * cosine + lower * sine], axis=-1)


def fold_maps(left_part, right_part):
    left_max, left_sum, left_out = left_part
    right_max, right_sum, right_out = right_part
    joint = jnp.maximum(left_max, right_max)
    left_scale = jnp.exp(left_max - joint)
    right_scale = jnp.exp(right_max - joint)
    return (
        joint,
        left_sum * left_scale + right_sum * right_scale,
        left_out * left_scale[..., None] + right_out * right_scale[..., None],
    )


def on_device(
    tokens,
    norm_gain,
    query_weight,
    key_weight,
    value_weight,
    lambda_head,
    head_gain,
    out_weight,
    cache_keys,
    cache_values,
    lengths,
):
    seq_count = tokens.shape[0]
    heads_loc = lambda_head.shape[0]
    token_block, gain_block = (
        lax.all_gather(tokens, "tp", axis=1, tiled=True),
        lax.all_gather(norm_gain, "tp", axis=0, tiled=True),
    )
    tok_float = token_block.astype(jnp.float32)
    scaled = (tok_float * gain_block.astype(jnp.float32)).astype(jnp.bfloat16)
    query_part = jnp.dot(scaled, query_weight, preferred_element_type=jnp.float32)
    key_part = jnp.dot(scaled, key_weight, preferred_element_type=jnp.float32)
    value_part = jnp.dot(scaled, value_weight, preferred_element_type=jnp.float32)
    local_squares = jnp.sum(tok_float * tok_float, axis=1)
    query_sum, key_sum, value_sum, row_squares = lax.psum(
        (query_part, key_part, value_part, local_squares), "kv"
    )
    inv_rms = lax.rsqrt(row_squares / D + 1e-06)[:, None]
    queries = rotate(
        (query_sum * inv_rms).reshape(seq_count, heads_loc, 2, HEAD_DIM), lengths
    ).astype(jnp.bfloat16)
    key_new = rotate(
        (key_sum * inv_rms).reshape(seq_count, heads_loc, 2, HEAD_DIM), lengths
    ).astype(jnp.bfloat16)
    value_new = (value_sum * inv_rms).astype(jnp.bfloat16).reshape(seq_count, heads_loc, VALUE_DIM)
    span_len = cache_keys.shape[1]
    positions = lax.axis_index("kv") * span_len + jnp.arange(span_len, dtype=jnp.int32)
    new_slot = positions[None, :] == lengths[:, None]
    before = positions[None, :] < lengths[:, None]
    visible = positions[None, :] <= lengths[:, None]
    score_scale = HEAD_DIM ** (-0.5)
    keys_four = cache_keys.reshape(seq_count, span_len, heads_loc, 2, HEAD_DIM)
    scores = (
        jnp.einsum("bhcd,bphcd->bhcp", queries, keys_four, preferred_element_type=jnp.float32)
        * score_scale
    )
    new_score = (
        jnp.einsum("bhcd,bhcd->bhc", queries, key_new, preferred_element_type=jnp.float32)
        * score_scale
    )
    scores = jnp.where(new_slot[:, None, None, :], new_score[..., None], scores)
    visible_four = visible[:, None, None, :]
    block_max = jnp.max(jnp.where(visible_four, scores, -1e30), axis=-1)
    weights = jnp.where(visible_four, jnp.exp(scores - block_max[..., None]), 0.0)
    block_sum = jnp.sum(weights, axis=-1)
    weights_low = weights.astype(jnp.bfloat16)
    cache_weights = jnp.where(before[:, None, None, :], weights_low, jnp.zeros((), jnp.bfloat16))
    values_four = cache_values.reshape(seq_count, span_len, heads_loc, VALUE_DIM)
    block_out = jnp.einsum(
        "bhcp,bphe->bhce", cache_weights, values_four, preferred_element_type=jnp.float32
    )
    weight_new = jnp.sum(
        jnp.where(new_slot[:, None, None, :], weights_low.astype(jnp.float32), 0.0), axis=-1
    )
    block_out = block_out + weight_new[..., None] * value_new.astype(jnp.float32)[:, :, None, :]
    row_max, weight_total, combined = merged((block_max, block_sum, block_out), "kv", fold_maps)
    map_out = combined / weight_total[..., None]
    difference = map_out[:, :, 0] - lambda_head[None, :, None] * map_out[:, :, 1]
    inv_head = lax.rsqrt(jnp.mean(difference * difference, axis=-1, keepdims=True) + 1e-05)
    attended = (
        (difference * inv_head * head_gain)
        .astype(jnp.bfloat16)
        .reshape(seq_count, heads_loc * VALUE_DIM)
    )
    log_sums = row_max + jnp.log(weight_total)
    partial_value = jnp.dot(attended, out_weight, preferred_element_type=jnp.float32)
    layer_out = lax.psum_scatter(
        partial_value.astype(jnp.bfloat16), "tp", scatter_dimension=1, tiled=True
    )
    return (layer_out, log_sums)


MESH = pl.DeviceIdType.MESH
LANES = 128
ROWS = 8


STEPS = 32767.0
MASS_LANE = 64


def stat_lanes(groups, heads):
    return groups * (2 * heads + 1)


def fused_kernel(
    n_kv,
    n_tp,
    tok_hbm,
    gain_hbm,
    wq_hbm,
    wk_hbm,
    wv_hbm,
    lam_hbm,
    hgain_hbm,
    wo_hbm,
    ck_hbm,
    cv_hbm,
    len_hbm,
    out_ref,
    log_ref,
    tok_buf,
    gain_buf,
    lam_ref,
    hgain_ref,
    len_ref,
    wq_buf,
    wk_buf,
    wv_buf,
    k_buf,
    v_buf,
    wo_buf,
    q_buf,
    q_stat,
    q_scale,
    q_rot,
    new_buf,
    new_stat,
    att_buf,
    att_stat,
    head_buf,
    log_buf,
    o_send,
    o_recv,
    own_sem,
    w_sem,
    kv_sem,
    wo_sem,
    tok_ss,
    tok_rs,
    q_ss,
    q_rs,
    qs_ss,
    qs_rs,
    new_ss,
    new_rs,
    ns_ss,
    ns_rs,
    att_ss,
    att_rs,
    as_ss,
    as_rs,
    head_ss,
    head_rs,
    log_ss,
    log_rs,
    o_ss,
    o_rs,
    plane_sem,
    all_sem,
):
    f32, bf16, i32, i16 = jnp.float32, jnp.bfloat16, jnp.int32, jnp.int16
    my_kv, my_tp = lax.axis_index("kv"), lax.axis_index("tp")
    seqs, tok_w = tok_hbm.shape
    span = ck_hbm.shape[1]
    vdim = VALUE_DIM
    heads = n_kv
    per_owner = heads // 2
    groups = seqs // ROWS
    out_w = out_ref.shape[1]
    first_owner = n_kv // 2 - 1
    low_side = my_kv <= first_owner
    is_owner = (my_kv == first_owner) | (my_kv == first_owner + 1)
    far_owner = jnp.where(low_side, 1, 0)
    stride = 2 * heads + 1

    def tp_at(offset):
        return lax.rem(my_tp + offset, n_tp)

    def kv_at(offset):
        return lax.rem(my_kv + offset, n_kv)

    def kv_peer(t):
        down = n_kv - 1 - t
        down = jnp.where(down <= my_kv, down - 1, down)
        up = jnp.where(t >= my_kv, t + 1, t)
        return jnp.where(low_side, down, up)

    def slot_head(i, far):
        owner = far if i % 2 == 0 else 1 - far
        return owner * per_owner + i // 2

    def remote(src, dst, ss, rs, axis, peer):
        return pltpu.make_async_remote_copy(
            src_ref=src, dst_ref=dst, send_sem=ss, recv_sem=rs, device_id={axis: peer}, device_id_type=MESH
        )

    def send(*args):
        copy = remote(*args)
        copy.start()
        return copy

    def load(src, dst, sem):
        copy = pltpu.make_async_copy(src, dst, sem)
        copy.start()
        return copy

    barrier = pltpu.get_barrier_semaphore()
    gate, leader = n_tp - 1, n_tp - 2
    is_gate = my_tp == gate

    def signal(sem, axis, peer):
        pl.semaphore_signal(sem, inc=1, device_id={axis: peer}, device_id_type=MESH)

    for t in range(n_tp):
        if t != gate:

            @pl.when(my_tp != t)
            def _(t=t):
                signal(barrier, "tp", t)

    tok_load = load(tok_hbm, tok_buf.at[my_tp], own_sem.at[0])
    gain_load = load(gain_hbm, gain_buf.at[my_tp], own_sem.at[1])
    len_load = load(len_hbm, len_ref, own_sem.at[2])
    lam_load = load(lam_hbm, lam_ref, own_sem.at[3])
    hgain_load = load(hgain_hbm, hgain_ref, own_sem.at[4])
    tok_load.wait()
    gain_load.wait()
    w_loads = [
        load(w, buf, w_sem.at[m])
        for m, (w, buf) in enumerate(((wq_hbm, wq_buf), (wk_hbm, wk_buf), (wv_hbm, wv_buf)))
    ]
    kv_loads = []
    for i in range(heads):
        cols = pl.ds(pl.multiple_of(slot_head(i, far_owner) * vdim, vdim), vdim)
        kv_loads.append(
            (
                load(ck_hbm.at[:, :, cols], k_buf.at[i], kv_sem.at[2 * i]),
                load(cv_hbm.at[:, :, cols], v_buf.at[i], kv_sem.at[2 * i + 1]),
            )
        )
    wo_loads = []
    for i in range(n_tp):
        cols = pl.ds(pl.multiple_of(tp_at(i + 1) * out_w, out_w), out_w)
        wo_loads.append(load(wo_hbm.at[:, cols], wo_buf.at[i], wo_sem.at[i]))


    @pl.when(jnp.logical_not(is_gate))
    def _():
        pl.semaphore_wait(barrier, n_tp - 1)

    @pl.when(my_tp == leader)
    def _():
        signal(plane_sem, "tp", gate)

    @pl.when(is_gate)
    def _():
        pl.semaphore_wait(plane_sem, 1)
        for offset in range(1, n_kv):
            signal(barrier, "kv", kv_at(offset))

    sends = []
    tok_copies = []
    for o in range(n_tp - 1, 0, -1):
        peer = tp_at(o)
        for m, buf in enumerate((tok_buf, gain_buf)):
            tok_copies.append(
                send(
                    buf.at[my_tp],
                    buf.at[my_tp],
                    tok_ss.at[2 * o - 2 + m],
                    tok_rs.at[2 * o - 2 + m],
                    "tp",
                    peer,
                )
            )
    sends += tok_copies

    @pl.when(is_gate)
    def _():
        pl.semaphore_wait(barrier, n_kv - 1)
        for t in range(n_tp):
            if t != gate:
                signal(all_sem, "tp", t)

    len_load.wait()
    lane_id = lax.broadcasted_iota(i32, (seqs, LANES), 1)
    row_id = lax.broadcasted_iota(i32, (seqs, LANES), 0)
    lens = jnp.zeros((seqs, LANES), i32)
    for b in range(seqs):
        lens = jnp.where(row_id == b, len_ref[b], lens)
    half = HEAD_DIM // 2
    upper = lane_id >= half
    freq_id = jnp.where(upper, lane_id - half, lane_id).astype(f32)
    angles = lens.astype(f32) * jnp.exp(freq_id * (-2.0 * math.log(500000.0) / HEAD_DIM))
    cosine = jnp.cos(angles)
    sine = jnp.sin(angles)
    sine = jnp.where(upper, sine, -sine)

    def rotated(x):
        return (x * cosine + pltpu.roll(x, half, 1) * sine).astype(bf16)

    lane = lax.broadcasted_iota(i32, (ROWS, LANES), 1)

    def packed(columns):
        tile = jnp.zeros((ROWS, LANES), f32)
        for at, column in columns:
            tile = jnp.where(lane == at, column, tile)
        return tile

    def coded(x):
        top = jnp.maximum(jnp.max(jnp.abs(x), axis=1, keepdims=True), 1e-30)
        code = jnp.round(x * (STEPS / top)).astype(i32).astype(i16)
        return code, top * (1.0 / STEPS)

    def rows_of(g):
        return slice(g * ROWS, (g + 1) * ROWS)

    def decoded(codes, tile, width, at):
        value = codes.astype(i32).astype(f32)
        pieces = []
        for g in range(groups):
            rows = []
            for c in range(width):
                scale = tile[:, g * stride + at + c : g * stride + at + c + 1]
                rows.append(value[rows_of(g), c * LANES : (c + 1) * LANES] * scale)
            pieces.append(jnp.concatenate(rows, axis=1))
        return jnp.concatenate(pieces, axis=0)

    for copy in tok_copies:
        copy.wait_recv()
    squares = jnp.zeros((seqs, 1), f32)
    scaled_parts = []
    for s in range(n_tp):
        tok = tok_buf[s].astype(f32)
        squares = squares + jnp.sum(tok * tok, axis=1, keepdims=True)
        gain = gain_buf[s].astype(f32)
        gain = jnp.concatenate([gain[r : r + 1] for r in range(tok_w // LANES)], axis=1)
        scaled_parts.append((tok * gain).astype(bf16))
    scaled = jnp.concatenate(scaled_parts, axis=1)

    w_loads[0].wait()
    for j in range(per_owner):
        columns = [(g * stride + 2 * heads, squares[rows_of(g)]) for g in range(groups)]
        for h in (j, per_owner + j):
            part = jnp.dot(scaled, wq_buf[:, h * vdim : (h + 1) * vdim], preferred_element_type=f32)
            for c in range(2):
                cols = slice(c * HEAD_DIM, (c + 1) * HEAD_DIM)
                code, scale = coded(part[:, cols])
                q_buf[my_kv, h, :, cols] = code
                columns += [(g * stride + 2 * h + c, scale[rows_of(g)]) for g in range(groups)]
        q_stat[my_kv, j] = packed(columns)
        if j == 0:

            @pl.when(jnp.logical_not(is_gate))
            def _():
                pl.semaphore_wait(all_sem, 1)

        for t in range(n_kv - 1):
            at = q_stat.at[my_kv, j]
            sends.append(send(at, at, qs_ss.at[t, j], qs_rs.at[my_kv, j], "kv", kv_peer(t)))
        for i in (2 * j, 2 * j + 1):
            for t in range(n_kv - 1):
                peer = kv_peer(t)
                h = slot_head(i, jnp.where(peer <= first_owner, 1, 0))
                at = q_buf.at[my_kv, h]
                sends.append(send(at, at, q_ss.at[i, t], q_rs.at[my_kv, h], "kv", peer))

    columns = []
    w_loads[1].wait()
    w_loads[2].wait()
    for m, w in enumerate((wk_buf, wv_buf)):
        part = jnp.dot(scaled, w[...], preferred_element_type=f32)
        for j in range(2 * heads):
            code, scale = coded(part[:, j * HEAD_DIM : (j + 1) * HEAD_DIM])
            lo = m * vdim + (j % 2) * HEAD_DIM
            new_buf[my_kv, j // 2, :, lo : lo + HEAD_DIM] = code
            columns.append((m, j, scale))
    for m in range(2):
        new_stat[my_kv, m] = packed(
            [(g * stride + j, scale[rows_of(g)]) for mm, j, scale in columns if mm == m for g in range(groups)]
        )

    def new_copies(h):
        at = new_buf.at[my_kv, h]
        return remote(at, at, new_ss.at[h], new_rs.at[my_kv, h], "kv", first_owner + h // per_owner)

    def new_stat_copy(w):
        at = new_stat.at[my_kv]
        return remote(at, at, ns_ss.at[w], ns_rs.at[my_kv], "kv", first_owner + w)

    score_scale = HEAD_DIM ** (-0.5)
    wide = ROWS * span
    col = lax.broadcasted_iota(i32, (2 * ROWS, wide), 1)
    row = lax.broadcasted_iota(i32, (2 * ROWS, wide), 0)
    start = (row % ROWS) * span
    masks = []
    for g in range(groups):
        len_g = lens[rows_of(g), 0:1]
        len_g = jnp.concatenate([len_g, len_g], axis=0)
        limit = jnp.minimum(len_g - my_kv * span, span)
        masks.append((col >= start) & (col - start < limit))
    lane_q = lax.broadcasted_iota(i32, (ROWS, vdim), 1)
    contract_last = (((1,), (1,)), ((), ()))

    def att_copies(i):
        h = slot_head(i, far_owner)
        owner = first_owner + (far_owner if i % 2 == 0 else 1 - far_owner)
        at, stat_at = att_buf.at[my_kv, h], att_stat.at[my_kv, h]
        return [
            remote(at, at, att_ss.at[i], att_rs.at[my_kv, h], "kv", owner),
            remote(stat_at, stat_at, as_ss.at[i], as_rs.at[my_kv, h], "kv", owner),
        ]

    for j in range(per_owner):
        for o in range(1, n_kv):
            peer = kv_at(o)
            at = q_stat.at[peer, j]
            remote(at, at, qs_ss.at[o - 1, j], qs_rs.at[peer, j], "kv", peer).wait_recv()
        if j == 0:
            inv_rms = []
            for g in range(groups):
                at = g * stride + 2 * heads
                total = q_stat[0, 0][:, at : at + 1]
                for s in range(1, n_kv):
                    total = total + q_stat[s, 0][:, at : at + 1]
                inv_rms.append(lax.rsqrt(total / (tok_w * n_tp * n_kv) + 1e-06))
            inv_rms = jnp.concatenate(inv_rms, axis=0)
        for i in (2 * j, 2 * j + 1):
            h = slot_head(i, far_owner)
            for s in range(n_kv):
                tile = pltpu.roll(q_stat[s, j], lax.rem(LANES - 2 * h, LANES), 1)
                for c in range(2):
                    scale = jnp.concatenate([tile[:, g * stride + c : g * stride + c + 1] for g in range(groups)], axis=0)
                    cols = slice(c * HEAD_DIM, (c + 1) * HEAD_DIM)
                    q_scale[i, s, :, cols] = jnp.broadcast_to(scale * inv_rms, (seqs, HEAD_DIM))

    def arrived(i):
        h = slot_head(i, far_owner)
        for o in range(1, n_kv):
            peer = kv_at(o)
            at = q_buf.at[peer, h]
            remote(at, at, q_ss.at[i, o - 1], q_rs.at[peer, h], "kv", peer).wait_recv()
        kv_loads[i][0].wait()
        kv_loads[i][1].wait()

    def attend(slots):
        jobs = [(i, g) for i in slots for g in range(groups)]
        queries, scores, tops, weights, masses, outs = {}, {}, {}, {}, {}, {}
        for i in slots:
            h = slot_head(i, far_owner)
            total = jnp.zeros((seqs, vdim), f32)
            for s in range(n_kv):
                total = total + q_buf[s, h].astype(i32).astype(f32) * q_scale[i, s]
            maps = [rotated(total[:, c * HEAD_DIM : (c + 1) * HEAD_DIM]) for c in range(2)]
            for c in range(2):
                q_rot[i, :, c * HEAD_DIM : (c + 1) * HEAD_DIM] = maps[c]
            queries[i] = jnp.concatenate([m.astype(f32) for m in maps], axis=1)
        for i, g in jobs:
            q_g = queries[i][rows_of(g)]
            lhs = jnp.concatenate(
                [jnp.where(lane_q < HEAD_DIM, q_g, 0.0), jnp.where(lane_q < HEAD_DIM, 0.0, q_g)], axis=0
            ).astype(bf16)
            keys = k_buf[i, rows_of(g)].reshape(wide, vdim)
            scores[i, g] = lax.dot_general(lhs, keys, contract_last, preferred_element_type=f32)
        for i, g in jobs:
            scores[i, g] = jnp.where(masks[g], scores[i, g] * score_scale, -1e30)
            tops[i, g] = jnp.max(scores[i, g], axis=1, keepdims=True)
        for i, g in jobs:
            weights[i, g] = jnp.where(masks[g], jnp.exp(scores[i, g] - tops[i, g]), 0.0)
            masses[i, g] = jnp.sum(weights[i, g], axis=1, keepdims=True)
        for i, g in jobs:
            values = v_buf[i, rows_of(g)].reshape(wide, vdim)
            outs[i, g] = jnp.dot(weights[i, g].astype(bf16), values, preferred_element_type=f32)
        for i in slots:
            h = slot_head(i, far_owner)
            stats = []
            for g in range(groups):
                out = outs[i, g].astype(bf16)
                for c in range(2):
                    part = slice(c * ROWS, (c + 1) * ROWS)
                    att_buf[my_kv, h, c * seqs + g * ROWS : c * seqs + (g + 1) * ROWS] = out[part]
                    stats.append((2 * g + c, tops[i, g][part]))
                    stats.append((MASS_LANE + 2 * g + c, masses[i, g][part]))
            att_stat[my_kv, h] = packed(stats)

    def deliver(i):
        if i % 2 == 0:
            for copy in att_copies(i):
                copy.start()
        else:

            @pl.when(jnp.logical_not(is_owner))
            def _():
                for copy in att_copies(i):
                    copy.start()

    turns = [(i, i + 1) for i in range(0, heads - 2, 2)] + [(heads - 2,), (heads - 1,)]
    for j, turn in enumerate(turns):
        for i in turn:
            arrived(i)
        if j == 0:
            for w in range(2):

                @pl.when(my_kv != first_owner + w)
                def _(w=w):
                    new_stat_copy(w).start()
                    for k in range(per_owner):
                        new_copies(w * per_owner + k).start()

        attend(turn)
        for i in turn:
            deliver(i)

    lam_load.wait()
    hgain_load.wait()

    def head_copies(h):
        at, log_at = head_buf.at[h], log_buf.at[h]
        made = []
        for o in range(1, n_kv):
            peer = kv_at(o)
            made.append(remote(at, at, head_ss.at[h, o - 1], head_rs.at[h], "kv", peer))
        for o in range(1, n_kv):
            peer = kv_at(o)
            made.append(remote(log_at, log_at, log_ss.at[h, o - 1], log_rs.at[h], "kv", peer))
        return made

    def own_head(w, j):
        return w * per_owner + j

    for w in range(2):

        @pl.when(my_kv == first_owner + w)
        def _(w=w):
            for o in range(1, n_kv):
                peer = kv_at(o)
                at = new_stat.at[peer]
                remote(at, at, ns_ss.at[w], ns_rs.at[peer], "kv", peer).wait_recv()
            new_tiles, new_values = [], []
            for j in range(per_owner):
                h = own_head(w, j)
                for o in range(1, n_kv):
                    peer = kv_at(o)
                    at = new_buf.at[peer, h]
                    remote(at, at, new_ss.at[h], new_rs.at[peer, h], "kv", peer).wait_recv()
                k_sum = jnp.zeros((seqs, vdim), f32)
                v_sum = jnp.zeros((seqs, vdim), f32)
                for s in range(n_kv):
                    codes = new_buf[s, h]
                    k_sum = k_sum + decoded(codes[:, :vdim], new_stat[s, 0], 2, 2 * h)
                    v_sum = v_sum + decoded(codes[:, vdim:], new_stat[s, 1], 2, 2 * h)
                k_sum = k_sum * inv_rms
                new_values.append((v_sum * inv_rms).astype(bf16).astype(f32))
                scores = []
                for c in range(2):
                    cols = slice(c * HEAD_DIM, (c + 1) * HEAD_DIM)
                    k_new = rotated(k_sum[:, cols]).astype(f32)
                    score = jnp.sum(q_rot[2 * j + 1, :, cols].astype(f32) * k_new, axis=1, keepdims=True)
                    scores += [(2 * g + c, score[rows_of(g)] * score_scale) for g in range(groups)]
                new_tiles.append(packed(scores))
            for j in range(per_owner):
                h = own_head(w, j)
                for o in range(1, n_kv):
                    peer = kv_at(o)
                    at, stat_at = att_buf.at[peer, h], att_stat.at[peer, h]
                    remote(at, at, att_ss.at[0], att_rs.at[peer, h], "kv", peer).wait_recv()
                    remote(stat_at, stat_at, as_ss.at[0], as_rs.at[peer, h], "kv", peer).wait_recv()
                row_max = new_tiles[j]
                for s in range(n_kv):
                    row_max = jnp.maximum(row_max, att_stat[s, h])
                new_weight = jnp.exp(new_tiles[j] - row_max)
                total = new_weight
                scales = []
                for s in range(n_kv):
                    tile = att_stat[s, h]
                    scale = jnp.exp(tile - row_max)
                    total = total + scale * pltpu.roll(tile, LANES - MASS_LANE, 1)
                    scales.append(scale)
                share = 1.0 / total
                share = share * jnp.where(lane % 2 == 0, 1.0, -lam_ref[h])
                new_share = new_weight * share
                shares = [scale * share for scale in scales]
                log_buf[h] = row_max + jnp.log(total)
                pieces = []
                for g in range(groups):
                    at = 2 * g
                    piece = (new_share[:, at : at + 1] + new_share[:, at + 1 : at + 2]) * new_values[j][rows_of(g)]
                    for s in range(n_kv):
                        for c in range(2):
                            dst = slice(c * seqs + g * ROWS, c * seqs + (g + 1) * ROWS)
                            piece = piece + shares[s][:, at + c : at + c + 1] * att_buf[s, h, dst].astype(f32)
                    pieces.append(piece)
                difference = jnp.concatenate(pieces, axis=0)
                inv_head = lax.rsqrt(jnp.mean(difference * difference, axis=1, keepdims=True) + 1e-05)
                head_buf[h] = (difference * inv_head * hgain_ref[...]).astype(bf16)
                for copy in head_copies(h):
                    copy.start()

    for copy in wo_loads:
        copy.wait()
    head_order = [w * per_owner + j for j in range(per_owner) for w in range(2)]
    parts = [None] * n_tp
    for h in head_order:

        @pl.when(my_kv != first_owner + h // per_owner)
        def _(h=h):
            at = head_buf.at[h]
            remote(at, at, head_ss.at[h, 0], head_rs.at[h], "kv", kv_at(1)).wait_recv()

        attended = head_buf[h]
        for i in range(n_tp):
            term = jnp.dot(attended, wo_buf[i, h * vdim : (h + 1) * vdim], preferred_element_type=f32)
            parts[i] = term if parts[i] is None else parts[i] + term
    o_copies = []
    for i in range(n_tp - 1):
        o_send[i] = parts[i].astype(bf16)
        o_copies.append(send(o_send.at[i], o_recv.at[i], o_ss.at[i], o_rs.at[i], "tp", tp_at(i + 1)))
    sends += o_copies

    for h in range(heads):

        @pl.when(my_kv != first_owner + h // per_owner)
        def _(h=h):
            at = log_buf.at[h]
            remote(at, at, log_ss.at[h, 0], log_rs.at[h], "kv", kv_at(1)).wait_recv()

    pieces = []
    for g in range(groups):
        piece = jnp.zeros((ROWS, LANES), f32)
        for h in range(heads):
            tile = pltpu.roll(log_buf[h], (2 * h - 2 * g) % LANES, 1)
            piece = jnp.where((lane // 2) == h, tile, piece)
        pieces.append(piece)
    logs = jnp.concatenate(pieces, axis=0).T
    for h in range(heads):
        log_ref[h] = logs[2 * h : 2 * h + 2]

    result = parts[n_tp - 1].astype(bf16).astype(f32)
    for i, copy in enumerate(o_copies):
        copy.wait_recv()
        result = result + o_recv[i].astype(f32)
    out_ref[...] = result.astype(bf16)

    for copy in sends:
        copy.wait_send()
    for i in range(heads):
        if i % 2 == 0:
            for copy in att_copies(i):
                copy.wait_send()
        else:

            @pl.when(jnp.logical_not(is_owner))
            def _(i=i):
                for copy in att_copies(i):
                    copy.wait_send()

    for w in range(2):

        @pl.when(my_kv != first_owner + w)
        def _(w=w):
            new_stat_copy(w).wait_send()
            for j in range(per_owner):
                new_copies(w * per_owner + j).wait_send()

        @pl.when(my_kv == first_owner + w)
        def _(w=w):
            for j in range(per_owner):
                for copy in head_copies(own_head(w, j)):
                    copy.wait_send()


def hand_out(layer_in, logs_in, layer_out, logs_out):
    layer_out[...] = layer_in[...]
    logs_out[...] = logs_in[...]


def fused(
    n_kv,
    n_tp,
    tokens,
    norm_gain,
    query_weight,
    key_weight,
    value_weight,
    lambda_head,
    head_gain,
    out_weight,
    cache_keys,
    cache_values,
    lengths,
):
    seqs, tok_w = tokens.shape
    span = cache_keys.shape[1]
    depth, width = query_weight.shape
    heads = lambda_head.shape[0]
    out_w = out_weight.shape[1] // n_tp
    bf16, f32, i16 = jnp.bfloat16, jnp.float32, jnp.int16
    dma = pltpu.SemaphoreType.DMA
    anyspace = pl.BlockSpec(memory_space=pl.ANY)
    vmem = pl.BlockSpec(memory_space=pltpu.VMEM)
    k1, t1 = n_kv - 1, n_tp - 1
    operands = [
        pltpu.with_memory_space_constraint(a, pltpu.HBM)
        for a in (
            tokens,
            norm_gain.reshape(tok_w // LANES, LANES),
            query_weight,
            key_weight,
            value_weight,
            lambda_head,
            head_gain.reshape(1, VALUE_DIM),
            out_weight,
            cache_keys,
            cache_values,
            lengths,
        )
    ]
    layer, logs = pl.pallas_call(
        functools.partial(fused_kernel, n_kv, n_tp),
        out_shape=(pltpu.VMEM((seqs, out_w), bf16), pltpu.VMEM((heads, 2, seqs), f32)),
        in_specs=[anyspace] * len(operands),
        out_specs=(vmem, vmem),
        scratch_shapes=[
            pltpu.VMEM((n_tp, seqs, tok_w), bf16),
            pltpu.VMEM((n_tp, tok_w // LANES, LANES), bf16),
            pltpu.SMEM(lambda_head.shape, f32),
            pltpu.VMEM((1, VALUE_DIM), f32),
            pltpu.SMEM(lengths.shape, jnp.int32),
            pltpu.VMEM((depth, width), bf16),
            pltpu.VMEM((depth, width), bf16),
            pltpu.VMEM((depth, width), bf16),
            pltpu.VMEM((heads, seqs, span, VALUE_DIM), bf16),
            pltpu.VMEM((heads, seqs, span, VALUE_DIM), bf16),
            pltpu.VMEM((n_tp, out_weight.shape[0], out_w), bf16),
            pltpu.VMEM((n_kv, heads, seqs, VALUE_DIM), i16),
            pltpu.VMEM((n_kv, heads // 2, ROWS, LANES), f32),
            pltpu.VMEM((heads, n_kv, seqs, VALUE_DIM), f32),
            pltpu.VMEM((heads, seqs, VALUE_DIM), bf16),
            pltpu.VMEM((n_kv, heads, seqs, 2 * VALUE_DIM), i16),
            pltpu.VMEM((n_kv, 2, ROWS, LANES), f32),
            pltpu.VMEM((n_kv, heads, 2 * seqs, VALUE_DIM), bf16),
            pltpu.VMEM((n_kv, heads, ROWS, LANES), f32),
            pltpu.VMEM((heads, seqs, VALUE_DIM), bf16),
            pltpu.VMEM((heads, ROWS, LANES), f32),
            pltpu.VMEM((t1, seqs, out_w), bf16),
            pltpu.VMEM((t1, seqs, out_w), bf16),
            dma((5,)),
            dma((3,)),
            dma((2 * heads,)),
            dma((n_tp,)),
            dma((2 * t1,)),
            dma((2 * t1,)),
            dma((heads, k1)),
            dma((n_kv, heads)),
            dma((k1, heads // 2)),
            dma((n_kv, heads // 2)),
            dma((heads,)),
            dma((n_kv, heads)),
            dma((2,)),
            dma((n_kv,)),
            dma((heads,)),
            dma((n_kv, heads)),
            dma((heads,)),
            dma((n_kv, heads)),
            dma((heads, k1)),
            dma((heads,)),
            dma((heads, k1)),
            dma((heads,)),
            dma((t1,)),
            dma((t1,)),
            pltpu.SemaphoreType.REGULAR,
            pltpu.SemaphoreType.REGULAR,
        ],
        compiler_params=pltpu.CompilerParams(
            collective_id=0, has_side_effects=True, vmem_limit_bytes=40 * 1024 * 1024
        ),
        name="decode_step",
    )(*operands)
    layer, logs = (pltpu.with_memory_space_constraint(a, pltpu.VMEM) for a in (layer, logs))
    layer, logs = pl.pallas_call(
        hand_out,
        out_shape=(
            jax.ShapeDtypeStruct((seqs, out_w), bf16),
            jax.ShapeDtypeStruct((heads, 2, seqs), f32),
        ),
        in_specs=(vmem, vmem),
        out_specs=(vmem, vmem),
        name="hand_out",
    )(layer, logs)
    return layer, logs.transpose(2, 0, 1)


def fits_fused(n_kv, n_tp, tokens, lambda_head, out_weight, cache_keys):
    seqs, tok_w = tokens.shape
    heads = lambda_head.shape[0]
    resident = 2 * (4 * out_weight.size + 2 * cache_keys.size)
    groups = seqs // ROWS
    return (
        heads == n_kv
        and n_kv > 2
        and n_kv % 2 == 0
        and n_tp > 1
        and seqs % ROWS == 0
        and tok_w % LANES == 0
        and (out_weight.shape[1] // n_tp) % LANES == 0
        and groups * (2 * heads + 1) <= LANES
        and 2 * groups <= MASS_LANE
        and cache_keys.shape[1] % 16 == 0
        and resident <= 24 * 1024 * 1024
    )


def step(*args):
    n_kv, n_tp = lax.axis_size("kv"), lax.axis_size("tp")
    tokens, lambda_head, out_weight, cache_keys = args[0], args[5], args[7], args[8]
    if fits_fused(n_kv, n_tp, tokens, lambda_head, out_weight, cache_keys):
        return fused(n_kv, n_tp, *args)
    return on_device(*args)


def solution(mesh):
    in_specs = (
        P("grp", ("kv", "tp")),
        P(("kv", "tp")),
        P("kv", "tp"),
        P("kv", "tp"),
        P("kv", "tp"),
        P("tp"),
        P(),
        P("tp", "kv"),
        P("grp", "kv", "tp"),
        P("grp", "kv", "tp"),
        P("grp"),
    )
    out_specs = (P("grp", ("kv", "tp")), P("grp", "tp", None))
    return jax.shard_map(
        step, mesh=mesh, in_specs=in_specs, out_specs=out_specs, check_vma=False
    )
```

time: 43.2 us -> 28.6 us (0.66)
  Pallas kernels: 38.4 us -> 27.8 us
  local copies, waits for them, and re-layouts: 3.89 us -> 0 us
    pallas_call x1 -> x2, Pallas kernels: 38.4 us -> 27.8 us  [the longest x1 27.2 us: fused(): pl.pallas_call(functools.partial(fused_kernel, n_kv, n_tp), out_shape=(pl...]
    slice x1 -> x0, local copies, waits for them, and re-layouts: 1.37 us -> none  [fused(): return (layer, logs[:, :2 * heads].reshape(seqs, heads, 2))]
    unnamed x1 -> x0, local copies, waits for them, and re-layouts: 1.31 us -> none
    reshape x1 -> x0, local copies, waits for them, and re-layouts: 1.22 us -> none  [fused(): norm_gain.reshape(1, tok_w)]
where the time goes in v1:
time: 28.6 us; the launch traced here: 28.4 us
  Pallas kernels  27.8 us (97%)
  between operations  0.64 us (2%)
    pallas_call x1, Pallas kernels, fused(): pl.pallas_call(functools.partial(fused_kernel, n_kv, n_tp), out_shape=(pl...  27.2 us
    pallas_call x1, Pallas kernels, fused(): pl.pallas_call(hand_out, out_shape=(jax.ShapeDtypeStruct((seqs, out_w), b...  0.6 us

profile of v1, /device:TPU:0, one launch (start us, length us, event | category | flops | bytes accessed | tf_op | source)
XLA Modules:
  0.0 28.4 jit_solution(12897755320181296228)
XLA Ops:
  0.6 27.2 %decode_step.1 = (bf16[24,256]{1,0:T(8,128)(2,1)S(1)}, f32[4,2,24]{2,1,0:T(2,128)S(1)}) custom-call(bf16[24,256]{1,0:T(8,128)(2,1)} %tok_hbm.1, bf16[2,128]{1,0:T(2,128)(2,1)} %bitcast.4, bf16[1024,1024]{1,0:T(8,128)(2,1)} %wq_hbm.1, bf16[1024,1024]{1,0:T(8,128)(2,1)} %wk_hbm.1, bf16[1024,1024]{1,0:T(8,128)(2,1)} %wv_hbm.1, f32[4]{0:T(128)} %lam_hbm.1, ...), custom_call_target="tpu_custom_call" | custom-call | tf_op jit(solution)/shard_map/decode_step/pallas_call | solution.py:772
  27.8 0.6 %hand_out.1 = (bf16[24,256]{1,0:T(8,128)(2,1)}, f32[4,2,24]{2,1,0:T(2,128)}) custom-call(bf16[24,256]{1,0:T(8,128)(2,1)S(1)} %get-tuple-element.6.layer_in, f32[4,2,24]{2,1,0:T(2,128)S(1)} %get-tuple-element.7.logs_in), custom_call_target="tpu_custom_call" | custom-call | tf_op jit(solution)/shard_map/hand_out/pallas_call | solution.py:834

commit v2 on v1

--- a/solution.py
+++ b/solution.py
@@ -139,11 +139,9 @@
 
 
 STEPS = 32767.0
+ROUND_UP = 1.0 + 2.0**-7
+SQUARE_LANES = 3
 MASS_LANE = 64
-
-
-def stat_lanes(groups, heads):
-    return groups * (2 * heads + 1)
 
 
 def fused_kernel(
@@ -225,7 +223,8 @@
     low_side = my_kv <= first_owner
     is_owner = (my_kv == first_owner) | (my_kv == first_owner + 1)
     far_owner = jnp.where(low_side, 1, 0)
-    stride = 2 * heads + 1
+    stride = 2 * heads + SQUARE_LANES
+    new_stride = 4 * heads
 
     def tp_at(offset):
         return lax.rem(my_tp + offset, n_tp)
@@ -363,8 +362,13 @@
 
     def coded(x):
         top = jnp.maximum(jnp.max(jnp.abs(x), axis=1, keepdims=True), 1e-30)
-        code = jnp.round(x * (STEPS / top)).astype(i32).astype(i16)
-        return code, top * (1.0 / STEPS)
+        scale = (top * (ROUND_UP / STEPS)).astype(bf16).astype(f32)
+        return jnp.round(x * (1.0 / scale)).astype(i32).astype(i16), scale
+
+    def thirds(x):
+        high = x.astype(bf16).astype(f32)
+        middle = (x - high).astype(bf16).astype(f32)
+        return high, middle, x - high - middle
 
     def rows_of(g):
         return slice(g * ROWS, (g + 1) * ROWS)
@@ -375,7 +379,7 @@
         for g in range(groups):
             rows = []
             for c in range(width):
-                scale = tile[:, g * stride + at + c : g * stride + at + c + 1]
+                scale = tile[:, g * new_stride + at + c : g * new_stride + at + c + 1]
                 rows.append(value[rows_of(g), c * LANES : (c + 1) * LANES] * scale)
             pieces.append(jnp.concatenate(rows, axis=1))
         return jnp.concatenate(pieces, axis=0)
@@ -393,8 +397,11 @@
     scaled = jnp.concatenate(scaled_parts, axis=1)
 
     w_loads[0].wait()
+    square_parts = thirds(squares)
     for j in range(per_owner):
-        columns = [(g * stride + 2 * heads, squares[rows_of(g)]) for g in range(groups)]
+        columns = [
+            (g * stride + 2 * heads + m, third[rows_of(g)]) for m, third in enumerate(square_parts) for g in range(groups)
+        ]
         for h in (j, per_owner + j):
             part = jnp.dot(scaled, wq_buf[:, h * vdim : (h + 1) * vdim], preferred_element_type=f32)
             for c in range(2):
@@ -402,7 +409,7 @@
                 code, scale = coded(part[:, cols])
                 q_buf[my_kv, h, :, cols] = code
                 columns += [(g * stride + 2 * h + c, scale[rows_of(g)]) for g in range(groups)]
-        q_stat[my_kv, j] = packed(columns)
+        q_stat[my_kv, j] = packed(columns).astype(bf16)
         if j == 0:
 
             @pl.when(jnp.logical_not(is_gate))
@@ -429,10 +436,9 @@
             lo = m * vdim + (j % 2) * HEAD_DIM
             new_buf[my_kv, j // 2, :, lo : lo + HEAD_DIM] = code
             columns.append((m, j, scale))
-    for m in range(2):
-        new_stat[my_kv, m] = packed(
-            [(g * stride + j, scale[rows_of(g)]) for mm, j, scale in columns if mm == m for g in range(groups)]
-        )
+    new_stat[my_kv] = packed(
+        [(g * new_stride + 2 * heads * m + j, scale[rows_of(g)]) for m, j, scale in columns for g in range(groups)]
+    ).astype(bf16)
 
     def new_copies(h):
         at = new_buf.at[my_kv, h]
@@ -465,24 +471,29 @@
             remote(stat_at, stat_at, as_ss.at[i], as_rs.at[my_kv, h], "kv", owner),
         ]
 
-    for j in range(per_owner):
+    def stats_arrived(j):
         for o in range(1, n_kv):
             peer = kv_at(o)
             at = q_stat.at[peer, j]
             remote(at, at, qs_ss.at[o - 1, j], qs_rs.at[peer, j], "kv", peer).wait_recv()
-        if j == 0:
-            inv_rms = []
-            for g in range(groups):
-                at = g * stride + 2 * heads
-                total = q_stat[0, 0][:, at : at + 1]
-                for s in range(1, n_kv):
-                    total = total + q_stat[s, 0][:, at : at + 1]
-                inv_rms.append(lax.rsqrt(total / (tok_w * n_tp * n_kv) + 1e-06))
-            inv_rms = jnp.concatenate(inv_rms, axis=0)
+
+    stats_arrived(0)
+    inv_rms = []
+    for g in range(groups):
+        total = jnp.zeros((ROWS, 1), f32)
+        for s in range(n_kv):
+            tile = q_stat[s, 0].astype(f32)
+            for m in range(SQUARE_LANES):
+                at = g * stride + 2 * heads + m
+                total = total + tile[:, at : at + 1]
+        inv_rms.append(lax.rsqrt(total / (tok_w * n_tp * n_kv) + 1e-06))
+    inv_rms = jnp.concatenate(inv_rms, axis=0)
+
+    def spread_scales(j):
         for i in (2 * j, 2 * j + 1):
             h = slot_head(i, far_owner)
             for s in range(n_kv):
-                tile = pltpu.roll(q_stat[s, j], lax.rem(LANES - 2 * h, LANES), 1)
+                tile = pltpu.roll(q_stat[s, j].astype(f32), lax.rem(LANES - 2 * h, LANES), 1)
                 for c in range(2):
                     scale = jnp.concatenate([tile[:, g * stride + c : g * stride + c + 1] for g in range(groups)], axis=0)
                     cols = slice(c * HEAD_DIM, (c + 1) * HEAD_DIM)
@@ -549,7 +560,11 @@
                     copy.start()
 
     turns = [(i, i + 1) for i in range(0, heads - 2, 2)] + [(heads - 2,), (heads - 1,)]
+    spread_scales(0)
     for j, turn in enumerate(turns):
+        if turn[0] % 2 == 0 and turn[0] > 0:
+            stats_arrived(turn[0] // 2)
+            spread_scales(turn[0] // 2)
         for i in turn:
             arrived(i)
         if j == 0:
@@ -601,8 +616,9 @@
                 v_sum = jnp.zeros((seqs, vdim), f32)
                 for s in range(n_kv):
                     codes = new_buf[s, h]
-                    k_sum = k_sum + decoded(codes[:, :vdim], new_stat[s, 0], 2, 2 * h)
-                    v_sum = v_sum + decoded(codes[:, vdim:], new_stat[s, 1], 2, 2 * h)
+                    tile = new_stat[s].astype(f32)
+                    k_sum = k_sum + decoded(codes[:, :vdim], tile, 2, 2 * h)
+                    v_sum = v_sum + decoded(codes[:, vdim:], tile, 2, 2 * (heads + h))
                 k_sum = k_sum * inv_rms
                 new_values.append((v_sum * inv_rms).astype(bf16).astype(f32))
                 scores = []
@@ -787,11 +803,11 @@
             pltpu.VMEM((heads, seqs, span, VALUE_DIM), bf16),
             pltpu.VMEM((n_tp, out_weight.shape[0], out_w), bf16),
             pltpu.VMEM((n_kv, heads, seqs, VALUE_DIM), i16),
-            pltpu.VMEM((n_kv, heads // 2, ROWS, LANES), f32),
+            pltpu.VMEM((n_kv, heads // 2, ROWS, LANES), bf16),
             pltpu.VMEM((heads, n_kv, seqs, VALUE_DIM), f32),
             pltpu.VMEM((heads, seqs, VALUE_DIM), bf16),
             pltpu.VMEM((n_kv, heads, seqs, 2 * VALUE_DIM), i16),
-            pltpu.VMEM((n_kv, 2, ROWS, LANES), f32),
+            pltpu.VMEM((n_kv, ROWS, LANES), bf16),
             pltpu.VMEM((n_kv, heads, 2 * seqs, VALUE_DIM), bf16),
             pltpu.VMEM((n_kv, heads, ROWS, LANES), f32),
             pltpu.VMEM((heads, seqs, VALUE_DIM), bf16),
@@ -857,7 +873,7 @@
         and seqs % ROWS == 0
         and tok_w % LANES == 0
         and (out_weight.shape[1] // n_tp) % LANES == 0
-        and groups * (2 * heads + 1) <= LANES
+        and groups * max(2 * heads + SQUARE_LANES, 4 * heads) <= LANES
         and 2 * groups <= MASS_LANE
         and cache_keys.shape[1] % 16 == 0
         and resident <= 24 * 1024 * 1024

time: 28.6 us -> 28.1 us (0.983)
  Pallas kernels: 27.8 us -> 27.2 us
    pallas_call x1, Pallas kernels: 27.2 us -> 26.6 us  [fused(): pl.pallas_call(functools.partial(fused_kernel, n_kv, n_tp), out_shape=(pl...]
where the time goes in v2:
time: 28.1 us; the launch traced here: 27.8 us
  Pallas kernels  27.2 us (97%)
  between operations  0.64 us (2%)
    pallas_call x1, Pallas kernels, fused(): pl.pallas_call(functools.partial(fused_kernel, n_kv, n_tp), out_shape=(pl...  26.6 us
    pallas_call x1, Pallas kernels, fused(): pl.pallas_call(hand_out, out_shape=(jax.ShapeDtypeStruct((seqs, out_w), b...  0.6 us

profile of v2, /device:TPU:0, one launch (start us, length us, event | category | flops | bytes accessed | tf_op | source)
XLA Modules:
  0.0 27.8 jit_solution(1976002628566109430)
XLA Ops:
  0.6 26.6 %decode_step.1 = (bf16[24,256]{1,0:T(8,128)(2,1)S(1)}, f32[4,2,24]{2,1,0:T(2,128)S(1)}) custom-call(bf16[24,256]{1,0:T(8,128)(2,1)} %tok_hbm.1, bf16[2,128]{1,0:T(2,128)(2,1)} %bitcast.4, bf16[1024,1024]{1,0:T(8,128)(2,1)} %wq_hbm.1, bf16[1024,1024]{1,0:T(8,128)(2,1)} %wk_hbm.1, bf16[1024,1024]{1,0:T(8,128)(2,1)} %wv_hbm.1, f32[4]{0:T(128)} %lam_hbm.1, ...), custom_call_target="tpu_custom_call" | custom-call | tf_op jit(solution)/shard_map/decode_step/pallas_call | solution.py:788
  27.2 0.6 %hand_out.1 = (bf16[24,256]{1,0:T(8,128)(2,1)}, f32[4,2,24]{2,1,0:T(2,128)}) custom-call(bf16[24,256]{1,0:T(8,128)(2,1)S(1)} %get-tuple-element.6.layer_in, f32[4,2,24]{2,1,0:T(2,128)S(1)} %get-tuple-element.7.logs_in), custom_call_target="tpu_custom_call" | custom-call | tf_op jit(solution)/shard_map/hand_out/pallas_call | solution.py:850

commit v3 on v2

--- a/solution.py
+++ b/solution.py
@@ -239,8 +239,8 @@
         return jnp.where(low_side, down, up)
 
     def slot_head(i, far):
-        owner = far if i % 2 == 0 else 1 - far
-        return owner * per_owner + i // 2
+        owner = far if i < per_owner else 1 - far
+        return owner * per_owner + i % per_owner
 
     def remote(src, dst, ss, rs, axis, peer):
         return pltpu.make_async_remote_copy(
@@ -398,33 +398,31 @@
 
     w_loads[0].wait()
     square_parts = thirds(squares)
-    for j in range(per_owner):
-        columns = [
-            (g * stride + 2 * heads + m, third[rows_of(g)]) for m, third in enumerate(square_parts) for g in range(groups)
-        ]
-        for h in (j, per_owner + j):
-            part = jnp.dot(scaled, wq_buf[:, h * vdim : (h + 1) * vdim], preferred_element_type=f32)
-            for c in range(2):
-                cols = slice(c * HEAD_DIM, (c + 1) * HEAD_DIM)
-                code, scale = coded(part[:, cols])
-                q_buf[my_kv, h, :, cols] = code
-                columns += [(g * stride + 2 * h + c, scale[rows_of(g)]) for g in range(groups)]
-        q_stat[my_kv, j] = packed(columns).astype(bf16)
-        if j == 0:
-
-            @pl.when(jnp.logical_not(is_gate))
-            def _():
-                pl.semaphore_wait(all_sem, 1)
-
+    columns = [
+        (g * stride + 2 * heads + m, third[rows_of(g)]) for m, third in enumerate(square_parts) for g in range(groups)
+    ]
+    for h in range(heads):
+        part = jnp.dot(scaled, wq_buf[:, h * vdim : (h + 1) * vdim], preferred_element_type=f32)
+        for c in range(2):
+            cols = slice(c * HEAD_DIM, (c + 1) * HEAD_DIM)
+            code, scale = coded(part[:, cols])
+            q_buf[my_kv, h, :, cols] = code
+            columns += [(g * stride + 2 * h + c, scale[rows_of(g)]) for g in range(groups)]
+    q_stat[my_kv] = packed(columns).astype(bf16)
+
+    @pl.when(jnp.logical_not(is_gate))
+    def _():
+        pl.semaphore_wait(all_sem, 1)
+
+    for t in range(n_kv - 1):
+        at = q_stat.at[my_kv]
+        sends.append(send(at, at, qs_ss.at[t], qs_rs.at[my_kv], "kv", kv_peer(t)))
+    for i in range(heads):
         for t in range(n_kv - 1):
-            at = q_stat.at[my_kv, j]
-            sends.append(send(at, at, qs_ss.at[t, j], qs_rs.at[my_kv, j], "kv", kv_peer(t)))
-        for i in (2 * j, 2 * j + 1):
-            for t in range(n_kv - 1):
-                peer = kv_peer(t)
-                h = slot_head(i, jnp.where(peer <= first_owner, 1, 0))
-                at = q_buf.at[my_kv, h]
-                sends.append(send(at, at, q_ss.at[i, t], q_rs.at[my_kv, h], "kv", peer))
+            peer = kv_peer(t)
+            h = slot_head(i, jnp.where(peer <= first_owner, 1, 0))
+            at = q_buf.at[my_kv, h]
+            sends.append(send(at, at, q_ss.at[i, t], q_rs.at[my_kv, h], "kv", peer))
 
     columns = []
     w_loads[1].wait()
@@ -464,36 +462,33 @@
 
     def att_copies(i):
         h = slot_head(i, far_owner)
-        owner = first_owner + (far_owner if i % 2 == 0 else 1 - far_owner)
+        owner = first_owner + (far_owner if i < per_owner else 1 - far_owner)
         at, stat_at = att_buf.at[my_kv, h], att_stat.at[my_kv, h]
         return [
             remote(at, at, att_ss.at[i], att_rs.at[my_kv, h], "kv", owner),
             remote(stat_at, stat_at, as_ss.at[i], as_rs.at[my_kv, h], "kv", owner),
         ]
 
-    def stats_arrived(j):
-        for o in range(1, n_kv):
-            peer = kv_at(o)
-            at = q_stat.at[peer, j]
-            remote(at, at, qs_ss.at[o - 1, j], qs_rs.at[peer, j], "kv", peer).wait_recv()
-
-    stats_arrived(0)
+    for o in range(1, n_kv):
+        peer = kv_at(o)
+        at = q_stat.at[peer]
+        remote(at, at, qs_ss.at[o - 1], qs_rs.at[peer], "kv", peer).wait_recv()
     inv_rms = []
     for g in range(groups):
         total = jnp.zeros((ROWS, 1), f32)
         for s in range(n_kv):
-            tile = q_stat[s, 0].astype(f32)
+            tile = q_stat[s].astype(f32)
             for m in range(SQUARE_LANES):
                 at = g * stride + 2 * heads + m
                 total = total + tile[:, at : at + 1]
         inv_rms.append(lax.rsqrt(total / (tok_w * n_tp * n_kv) + 1e-06))
     inv_rms = jnp.concatenate(inv_rms, axis=0)
 
-    def spread_scales(j):
-        for i in (2 * j, 2 * j + 1):
+    def spread_scales(slots):
+        for i in slots:
             h = slot_head(i, far_owner)
             for s in range(n_kv):
-                tile = pltpu.roll(q_stat[s, j].astype(f32), lax.rem(LANES - 2 * h, LANES), 1)
+                tile = pltpu.roll(q_stat[s].astype(f32), lax.rem(LANES - 2 * h, LANES), 1)
                 for c in range(2):
                     scale = jnp.concatenate([tile[:, g * stride + c : g * stride + c + 1] for g in range(groups)], axis=0)
                     cols = slice(c * HEAD_DIM, (c + 1) * HEAD_DIM)
@@ -549,7 +544,7 @@
             att_stat[my_kv, h] = packed(stats)
 
     def deliver(i):
-        if i % 2 == 0:
+        if i < per_owner:
             for copy in att_copies(i):
                 copy.start()
         else:
@@ -559,12 +554,9 @@
                 for copy in att_copies(i):
                     copy.start()
 
-    turns = [(i, i + 1) for i in range(0, heads - 2, 2)] + [(heads - 2,), (heads - 1,)]
-    spread_scales(0)
+    turns = [(i,) for i in range(heads)]
+    spread_scales(range(heads))
     for j, turn in enumerate(turns):
-        if turn[0] % 2 == 0 and turn[0] > 0:
-            stats_arrived(turn[0] // 2)
-            spread_scales(turn[0] // 2)
         for i in turn:
             arrived(i)
         if j == 0:
@@ -625,7 +617,7 @@
                 for c in range(2):
                     cols = slice(c * HEAD_DIM, (c + 1) * HEAD_DIM)
                     k_new = rotated(k_sum[:, cols]).astype(f32)
-                    score = jnp.sum(q_rot[2 * j + 1, :, cols].astype(f32) * k_new, axis=1, keepdims=True)
+                    score = jnp.sum(q_rot[per_owner + j, :, cols].astype(f32) * k_new, axis=1, keepdims=True)
                     scores += [(2 * g + c, score[rows_of(g)] * score_scale) for g in range(groups)]
                 new_tiles.append(packed(scores))
             for j in range(per_owner):
@@ -714,7 +706,7 @@
     for copy in sends:
         copy.wait_send()
     for i in range(heads):
-        if i % 2 == 0:
+        if i < per_owner:
             for copy in att_copies(i):
                 copy.wait_send()
         else:
@@ -803,7 +795,7 @@
             pltpu.VMEM((heads, seqs, span, VALUE_DIM), bf16),
             pltpu.VMEM((n_tp, out_weight.shape[0], out_w), bf16),
             pltpu.VMEM((n_kv, heads, seqs, VALUE_DIM), i16),
-            pltpu.VMEM((n_kv, heads // 2, ROWS, LANES), bf16),
+            pltpu.VMEM((n_kv, ROWS, LANES), bf16),
             pltpu.VMEM((heads, n_kv, seqs, VALUE_DIM), f32),
             pltpu.VMEM((heads, seqs, VALUE_DIM), bf16),
             pltpu.VMEM((n_kv, heads, seqs, 2 * VALUE_DIM), i16),
@@ -822,8 +814,8 @@
             dma((2 * t1,)),
             dma((heads, k1)),
             dma((n_kv, heads)),
-            dma((k1, heads // 2)),
-            dma((n_kv, heads // 2)),
+            dma((k1,)),
+            dma((n_kv,)),
             dma((heads,)),
             dma((n_kv, heads)),
             dma((2,)),

time: 28.1 us -> 27.7 us (0.986)
  Pallas kernels: 27.2 us -> 26.8 us
    pallas_call x1, Pallas kernels: 26.6 us -> 26.2 us  [fused(): pl.pallas_call(functools.partial(fused_kernel, n_kv, n_tp), out_shape=(pl...]
where the time goes in v3:
time: 27.7 us; the launch traced here: 27.5 us
  Pallas kernels  26.8 us (97%)
  between operations  0.64 us (2%)
    pallas_call x1, Pallas kernels, fused(): pl.pallas_call(functools.partial(fused_kernel, n_kv, n_tp), out_shape=(pl...  26.2 us
    pallas_call x1, Pallas kernels, fused(): pl.pallas_call(hand_out, out_shape=(jax.ShapeDtypeStruct((seqs, out_w), b...  0.6 us

profile of v3, /device:TPU:0, one launch (start us, length us, event | category | flops | bytes accessed | tf_op | source)
XLA Modules:
  0.0 27.5 jit_solution(10681392122458435711)
XLA Ops:
  0.6 26.2 %decode_step.1 = (bf16[24,256]{1,0:T(8,128)(2,1)S(1)}, f32[4,2,24]{2,1,0:T(2,128)S(1)}) custom-call(bf16[24,256]{1,0:T(8,128)(2,1)} %tok_hbm.1, bf16[2,128]{1,0:T(2,128)(2,1)} %bitcast.4, bf16[1024,1024]{1,0:T(8,128)(2,1)} %wq_hbm.1, bf16[1024,1024]{1,0:T(8,128)(2,1)} %wk_hbm.1, bf16[1024,1024]{1,0:T(8,128)(2,1)} %wv_hbm.1, f32[4]{0:T(128)} %lam_hbm.1, ...), custom_call_target="tpu_custom_call" | custom-call | tf_op jit(solution)/shard_map/decode_step/pallas_call | solution.py:780
  26.9 0.6 %hand_out.1 = (bf16[24,256]{1,0:T(8,128)(2,1)}, f32[4,2,24]{2,1,0:T(2,128)}) custom-call(bf16[24,256]{1,0:T(8,128)(2,1)S(1)} %get-tuple-element.6.layer_in, f32[4,2,24]{2,1,0:T(2,128)S(1)} %get-tuple-element.7.logs_in), custom_call_target="tpu_custom_call" | custom-call | tf_op jit(solution)/shard_map/hand_out/pallas_call | solution.py:842
